TPU v7x, 256 devices: a whole 4x4x8 slice. The times are simulated.
256 devices in a mesh: ep: 64 (over z, y, core), tp: 4 (over x).
Axes of the slice: x: 4, y: 4, z: 8, core: 2. Of those that a mesh axis runs over, the one named last changes fastest.
Arguments:
- queries: bfloat16 [12288, 8, 128], P('ep', 'tp'), may hold values from -140 to 140
- keys: bfloat16 [12288, 4, 128], P('ep', 'tp'), may hold values from -6 to 6
- values: bfloat16 [12288, 4, 128], P('ep', 'tp'), may hold values from -6 to 6
- mix_scale: float32 [8], P('tp'), may hold values from 0.3 to 0.8
- head_gain: float32 [128], replicated, may hold values from 0.1 to 1.9
- out_weight: bfloat16 [8, 128, 2048], P('tp'), may hold values from -0.1875 to 0.1875
- moe_input: bfloat16 [24576, 2048], P(('ep', 'tp')), may hold values from -6 to 6
- norm_gain: float32 [2048], replicated, may hold values from 0.1 to 1.9
- routes: int32 [24576, 2], P(('ep', 'tp')), may hold values from 0 to 63, all different within a row; in each aligned block of 96 rows (0 to 95, 96 to 191, ...) at most 4 rows name the same one
- route_weights: float32 [24576, 2], P(('ep', 'tp')), may hold values from 0.2 to 1
- gate_weight: bfloat16 [64, 2048, 3584], P('ep', None, 'tp'), may hold values from -0.125 to 0.125
- up_weight: bfloat16 [64, 2048, 3584], P('ep', None, 'tp'), may hold values from -0.125 to 0.125
- down_weight: bfloat16 [64, 3584, 2048], P('ep', 'tp'), may hold values from -0.09375 to 0.09375
Outputs:
- attn_out: bfloat16 [12288, 2048], P(('ep', 'tp'))
- moe_out: bfloat16 [24576, 2048], P(('ep', 'tp'))
Inputs may be any that keep to these rules, and one draw needn't show every extreme that they name: `routes`: the 2 experts of a row differ. In each aligned block of 96 rows (the rows of one device) no expert is named by more than 4 rows, and in some blocks an expert is named by exactly 4 rows.
All inputs are finite; a program needn't handle non-finite values.
Results may differ from a plain program's by a relative error of at most 0.014.
Values may be sent and summed in bfloat16 or wider, within the bound.
A program may use at most 128 MiB of HBM per device.

v0:
```python
import math
import jax
import jax.numpy as jnp
from jax import lax
from jax.sharding import Mesh
from jax.sharding import PartitionSpec as P

EP = ("ep_0", "ep_1", "ep_2")
EP_TP = ("ep_0", "ep_1", "ep_2", "tp")
NEG_LARGE = -1e30


def joined_along(tiles, dim):
    tiles = jnp.moveaxis(tiles, 0, dim)
    lengths = tiles.shape
    return tiles.reshape(*lengths[:dim], lengths[dim] * lengths[dim + 1], *lengths[dim + 2 :])


def gather_in_order(value, axes, order):
    tiles = value[None]
    for k in order:
        tiles = lax.all_gather(tiles, axes[k], axis=0, tiled=True)
    current = [lax.axis_size(axes[k]) for k in reversed(order)]
    tiles = tiles.reshape(*current, *value.shape)
    turned = sorted(range(len(order)), key=lambda place: order[len(order) - 1 - place])
    return tiles.transpose(*turned, *range(len(order), tiles.ndim)).reshape(-1, *value.shape)


def gathered_by_axis(value, axes, order, dim):
    return joined_along(gather_in_order(value, axes, order), dim)


def split_up(value, dim, peers):
    before, after = (value.shape[:dim], value.shape[dim + 1 :])
    return jnp.moveaxis(value.reshape(*before, peers, -1, *after), dim, 0)


def summed_on_arrival(value, axis, dim):
    peers = lax.axis_size(axis)
    tiles = lax.all_to_all(split_up(value, dim, peers), axis, 0, 0, tiled=True)
    return jnp.sum(tiles.astype(jnp.float32), axis=0)


def attend_update(running, query_set, positions, key_block, value_block, key_anchor, scaling):
    row_peak, totals, numerator = running
    span = key_block.shape[0]
    scores = (
        jnp.einsum("tkgmd,skmd->kgmts", query_set, key_block, preferred_element_type=jnp.float32)
        * scaling
    )
    visible = (key_anchor + jnp.arange(span, dtype=jnp.int32))[None, :] <= positions[:, None]
    scores = jnp.where(visible, scores, NEG_LARGE)
    new_peak = jnp.maximum(row_peak, jnp.max(scores, axis=-1))
    weights = jnp.where(visible, jnp.exp(scores - new_peak[..., None]), 0.0)
    factor = jnp.exp(row_peak - new_peak)
    totals = totals * factor + jnp.sum(weights, axis=-1)
    numerator = numerator * factor[..., None] + jnp.einsum(
        "rnouf,frj->rnouj",
        weights.astype(jnp.bfloat16),
        value_block,
        preferred_element_type=jnp.float32,
    )
    return (new_peak, totals, numerator)


def body(
    queries,
    keys,
    values,
    mix_scale,
    head_gain,
    out_weight,
    moe_input,
    norm_gain,
    routes,
    route_weights,
    gate_weight,
    up_weight,
    down_weight,
):
    rows_here = queries.shape[0]
    key_heads = keys.shape[1]
    head_count = queries.shape[1]
    group_size = head_count // key_heads
    head_dim = queries.shape[2] // 2
    value_dim = values.shape[2]
    ep_size = lax.axis_size(EP)
    own_start = lax.axis_index(EP) * rows_here
    grouped = queries.reshape(rows_here, key_heads, group_size, 2, head_dim)
    own_positions = own_start + jnp.arange(rows_here, dtype=jnp.int32)
    query_sets = ((grouped, own_positions),)
    scaling = 1.0 / math.sqrt(head_dim)

    def empty_state(row_total):
        return (
            jnp.full((key_heads, group_size, 2, row_total), NEG_LARGE, jnp.float32),
            jnp.zeros((key_heads, group_size, 2, row_total), jnp.float32),
            jnp.zeros((key_heads, group_size, 2, row_total, value_dim), jnp.float32),
        )

    initial = tuple((empty_state(entry[0].shape[0]) for entry in query_sets))
    key_rows = gathered_by_axis(keys, EP, (1, 0, 2), 0)
    value_rows = gathered_by_axis(values, EP, (1, 0, 2), 0)
    length = key_rows.shape[0]
    span = length
    while span > 1024 and span % 2 == 0:
        span = span // 2
    key_rows = key_rows.reshape(length, key_heads, 2, head_dim)

    def sweep(step_id, states):
        anchor = step_id * span
        key_block = lax.dynamic_slice_in_dim(key_rows, step_id * span, span, 0)
        value_block = lax.dynamic_slice_in_dim(value_rows, step_id * span, span, 0)
        updated = []
        for (query_set, positions), status in zip(query_sets, states):

            def advance(current):
                return attend_update(
                    current, query_set, positions, key_block, value_block, anchor, scaling
                )

            def unchanged(current):
                return current

            updated.append(lax.cond(anchor <= positions[-1], advance, unchanged, status))
        return tuple(updated)

    folded = lax.fori_loop(0, length // span, sweep, initial)
    mixing = mix_scale.reshape(key_heads, group_size, 1, 1)
    outputs = []
    for status in folded:
        row_peak, totals, numerator = status
        blended = numerator[:, :, 0] / totals[:, :, 0, :, None] - mixing * (
            numerator[:, :, 1] / totals[:, :, 1, :, None]
        )
        normed = (
            blended
            * lax.rsqrt(jnp.mean(blended * blended, axis=-1, keepdims=True) + 1e-05)
            * head_gain
        )
        outputs.append(
            jnp.transpose(normed.astype(jnp.bfloat16), (2, 0, 1, 3)).reshape(
                -1, head_count * value_dim
            )
        )
    head_flat = outputs[0]
    weight_flat = out_weight.reshape(head_count * value_dim, -1)
    widened = moe_input.astype(jnp.float32)
    normed_in = (
        widened * lax.rsqrt(jnp.mean(widened * widened, axis=-1, keepdims=True) + 1e-06) * norm_gain
    ).astype(jnp.bfloat16)
    tok_count = moe_input.shape[0]
    top_count = routes.shape[1]
    experts = ep_size * gate_weight.shape[0]
    capacity = max(2, 3 * top_count * tok_count // (2 * experts))
    flattened = routes.reshape(-1)
    one_hot = (flattened[:, None] == jnp.arange(experts, dtype=jnp.int32)[None, :]).astype(
        jnp.int32
    )
    before = jnp.cumsum(one_hot, axis=0) - one_hot
    ranking = jnp.sum(before * one_hot, axis=1)
    slot_ids = (flattened * capacity + ranking).reshape(tok_count, top_count)
    slot_total = experts * capacity
    dispatch = jnp.any(
        jnp.arange(slot_total, dtype=jnp.int32)[:, None, None] == slot_ids[None], axis=2
    ).astype(jnp.bfloat16)
    outbound = jnp.dot(dispatch, normed_in, preferred_element_type=jnp.float32).astype(jnp.bfloat16)
    received = lax.all_to_all(outbound, EP, split_axis=0, concat_axis=0, tiled=True)
    inputs = lax.all_gather(received, "tp", axis=0, tiled=True)
    gate_proj = jnp.dot(inputs, gate_weight[0], preferred_element_type=jnp.float32)
    up_proj = jnp.dot(inputs, up_weight[0], preferred_element_type=jnp.float32)
    hidden_all = (jax.nn.silu(gate_proj) * up_proj).astype(jnp.bfloat16)
    attn_out = summed_on_arrival(
        jnp.dot(head_flat, weight_flat, preferred_element_type=jnp.float32).astype(jnp.bfloat16),
        "tp",
        0,
    ).astype(jnp.bfloat16)
    expert_out = summed_on_arrival(
        jnp.dot(hidden_all, down_weight[0], preferred_element_type=jnp.float32).astype(
            jnp.bfloat16
        ),
        "tp",
        0,
    ).astype(jnp.bfloat16)
    returned_rows = lax.all_to_all(expert_out, EP, split_axis=0, concat_axis=0, tiled=True)
    picked = jnp.take(returned_rows, slot_ids, axis=0)
    moe_out = jnp.sum(route_weights[:, :, None] * picked.astype(jnp.float32), axis=1).astype(
        jnp.bfloat16
    )
    return (attn_out, moe_out)


def solution(mesh):
    split = Mesh(mesh.devices.reshape(8, 4, 2, mesh.shape["tp"]), ("ep_0", "ep_1", "ep_2", "tp"))
    placed = (
        P(EP, "tp", None),
        P(EP, "tp", None),
        P(EP, "tp", None),
        P("tp"),
        P(),
        P("tp", None, None),
        P(EP_TP, None),
        P(),
        P(EP_TP, None),
        P(EP_TP, None),
        P(EP, None, "tp"),
        P(EP, None, "tp"),
        P(EP, "tp", None),
    )
    return jax.shard_map(
        body,
        mesh=split,
        in_specs=placed,
        out_specs=(P(EP_TP, None), P(EP_TP, None)),
        check_vma=False,
    )
```

profile of v0, /device:TPU:1, one launch (start us, length us, event | category | flops | bytes accessed | tf_op | source)
XLA Modules:
  0.0 368.3 jit_solution(15211746906782629320)
XLA Ops:
  7.2 12.6 %all-gather = bf16[768,1,128]{2,0,1:T(8,128)(2,1)} all-gather(bf16[192,1,128]{2,0,1:T(8,128)(2,1)} %param.18), channel_id=2, replica_groups=mesh['ep_0'=8,'ep_1'=4,'ep_2'=2,'tp'=4] {'ep_1'}, dimensions={0}, use_global_device_ids=true | all-gather | bytes 245760 | tf_op jit(solution)/shard_map/all_gather | solution.py:22
  19.9 10.2 %all-gather.1 = bf16[768,1,128]{2,0,1:T(8,128)(2,1)} all-gather(bf16[192,1,128]{2,0,1:T(8,128)(2,1)} %param.19), channel_id=3, replica_groups=mesh['ep_0'=8,'ep_1'=4,'ep_2'=2,'tp'=4] {'ep_1'}, dimensions={0}, use_global_device_ids=true | all-gather | bytes 245760 | tf_op jit(solution)/shard_map/all_gather | solution.py:22
  30.2 0.8 copy.86
  31.1 0.6 reduce-window.6
  32.3 0.7 compare_and_fusion
  33.1 1.2 fusion.22
  34.3 1.5 convolution_convert_fusion.1
  36.3 47.2 %all_to_all.34 = bf16[64,4,2048]{2,1,0:T(4,128)(2,1)S(1)} all-to-all(bf16[64,4,2048]{2,1,0:T(4,128)(2,1)S(1)} %all_to_all.23), channel_id=1, replica_groups=mesh['ep_0'=8,'ep_1'=4,'ep_2'=2,'tp'=4] {'ep_0','ep_1','ep_2'}, dimensions={0} | all-to-all | bytes 2097152 | tf_op jit(solution)/shard_map/all_to_all | solution.py:168
  83.5 1.1 all_to_all.25
  85.2 23.4 %all-gather.12.cloned.1.call-done = bf16[32,192,1,128]{3,1,2,0:T(8,128)(2,1)} async-done(((bf16[4,192,1,128]{3,1,2,0:T(8,128)(2,1)}), bf16[32,192,1,128]{3,1,2,0:T(8,128)(2,1)}) %all-gather.12.cloned.1.call-update) | async-done | bytes 1572880 | tf_op jit(solution)/shard_map/all_gather | solution.py:22
  108.7 54.8 %all-gather.16.cloned.1.call-done = bf16[1024,2048]{1,0:T(8,128)(2,1)} async-done(((bf16[256,2048]{1,0:T(8,128)(2,1)}), bf16[1024,2048]{1,0:T(8,128)(2,1)}) %all-gather.16.cloned.1.call-update) | async-done | bytes 4194320 | tf_op jit(solution)/shard_map/all_gather | solution.py:169
  163.5 7.5 %fusion.16 = f32[1024,896]{1,0:T(8,128)S(1)} fusion(bf16[1024,2048]{1,0:T(8,128)(2,1)} %all-gather.16.cloned.1.call-done, bf16[1,2048,896]{2,1,0:T(8,128)(2,1)} %param.28), kind=kOutput, calls=%fused_computation.26 | convolution fusion | flops 3758096384 | bytes 11534336 | tf_op jit(solution)/shard_map/dot_general | solution.py:171
  171.0 4.7 %multiply_convert_fusion = bf16[1024,896]{1,0:T(8,128)(2,1)S(1)} fusion(f32[1024,896]{1,0:T(8,128)S(1)} %fusion.16, bf16[1024,2048]{1,0:T(8,128)(2,1)S(1)} %copy-done.5, bf16[1,2048,896]{2,1,0:T(8,128)(2,1)S(1)} %copy-done.6), kind=kOutput, calls=%fused_computation.30 | convolution fusion | flops 3763601408 | bytes 13369344 | tf_op jit(solution)/shard_map/dot_general | solution.py:170
  175.8 6.1 %convolution_convert_fusion = bf16[1024,2048]{1,0:T(8,128)(2,1)} fusion(bf16[1024,896]{1,0:T(8,128)(2,1)S(1)} %multiply_convert_fusion, bf16[1,896,2048]{2,1,0:T(8,128)(2,1)S(1)} %copy-done.7), kind=kOutput, calls=%fused_computation.24 | convolution fusion | flops 3760193536 | bytes 9699328 | tf_op jit(solution)/shard_map/dot_general | solution.py:179
  181.9 5.1 %all-to-all-start.2 = ((bf16[4,256,2048]{2,1,0:T(8,128)(2,1)}), bf16[4,256,2048]{2,1,0:T(8,128)(2,1)}, u32[]{:S(2)}, u32[]{:S(2)}) async-start(bf16[4,256,2048]{2,1,0:T(8,128)(2,1)} %bitcast.121), calls=%async_computation.2 | async-start | bytes 8388608 | tf_op jit(solution)/shard_map/all_to_all | solution.py:40
  187.2 11.2 %copy.79 = bf16[8,4,2,192,1,128]{3,2,1,0,5,4:T(2,128)(2,1)} copy(bf16[8,4,2,192,1,128]{5,3,1,0,2,4:T(8,128)(2,1)} %bitcast.122) | data formatting | bytes 6291456 | tf_op jit(solution)/shard_map/transpose | solution.py:26
  198.4 9.9 %reshape_reshape_reshape.3 = bf16[12288,1,2,64]{0,3,2,1:T(8,128)(2,1)} reshape(bf16[8,4,2,192,1,128]{3,2,1,0,5,4:T(2,128)(2,1)} %copy.79) | data formatting | bytes 6291456 | tf_op jit(solution)/shard_map/reshape;reshape;reshape | solution.py:108
  208.4 3.9 %copy.81 = bf16[8,4,2,192,1,128]{5,3,2,1,0,4:T(8,128)(2,1)} copy(bf16[8,4,2,192,1,128]{5,3,1,0,2,4:T(8,128)(2,1)} %bitcast.124) | data formatting | bytes 6291456 | tf_op jit(solution)/shard_map/transpose | solution.py:26
  212.3 24.4 %while.17 = (s32[]{:T(128)}, f32[1,2,2,192]{3,1,2,0:T(2,128)S(1)}, f32[1,2,2,192]{3,1,2,0:T(2,128)S(1)}, f32[1,2,2,192,128]{4,3,2,1,0:T(8,128)S(1)}, s32[192]{0:...) while((s32[]{:T(128)}, f32[1,2,2,192]{3,1,2,0:T(2,128)S(1)}, ...), condition=%wide.region_5.6_spmd, body=%wide.region_0.5_spmd.sunk | while | flops 232147968 | bytes 8857645 | solution.py:128
  212.4 0.6 slice.57
  213.6 4.3 %conditional.2 = ((f32[1,2,2,192]{3,1,2,0:T(2,128)S(1)}, f32[1,2,2,192]{3,1,2,0:T(2,128)S(1)}, f32[1,2,2,192,128]{4,3,2,1,0:T(8,128)S(1)})) conditional(s32[]{:T(128)} %convert_element_type.91, (f32[1,2,2,192]{3,1,2,0:T(2,128)S(1)}, f32[1,2,2,192]{3,1,2,0:T(2,128)S(1)}, f32[1,2,2,192,128]{4,3,2,1,0:T(8,128)S(1)}) %tuple.61, (s32[]{:T(128)}, ...), branch_computations={%region_1.0_spmd, %region_2.4_spmd} | conditional | flops 232147968 | bytes 8857422 | solution.py:125
  213.8 1.6 fusion
  215.4 0.9 fusion.4
  216.3 1.5 fusion.3
  217.9 0.6 slice.57
  219.1 0.6 slice.57
  220.4 0.6 slice.57
  221.7 0.6 slice.57
  222.9 0.6 slice.57
  224.2 0.6 slice.57
  225.4 0.6 slice.57
  226.7 0.6 slice.57
  227.9 0.6 slice.57
  229.2 0.6 slice.57
  230.4 0.6 slice.57
  233.0 0.6 slice.57
  234.2 0.6 slice.57
  235.5 0.6 slice.57
  237.3 1.3 convolution_convert_fusion.2
  238.6 4.0 %all-to-all-start = ((bf16[4,48,2048]{2,1,0:T(8,128)(2,1)}), bf16[4,48,2048]{2,1,0:T(8,128)(2,1)S(1)}, u32[]{:S(2)}, u32[]{:S(2)}) async-start(bf16[4,48,2048]{2,1,0:T(8,128)(2,1)} %bitcast.30), calls=%async_computation | async-start | bytes 1572864 | tf_op jit(solution)/shard_map/all_to_all | solution.py:40
  242.6 3.1 reduce_sum.78
  245.7 1.2 all_to_all.27
  246.9 6.6 %all-to-all-done = bf16[4,48,2048]{2,1,0:T(8,128)(2,1)S(1)} async-done(((bf16[4,48,2048]{2,1,0:T(8,128)(2,1)}), bf16[4,48,2048]{2,1,0:T(8,128)(2,1)S(1)}, u32[]{:S(2)}, u32[]{:S(2)}) %all-to-all-start) | async-done | bytes 786464 | tf_op jit(solution)/shard_map/all_to_all | solution.py:40
  253.5 74.0 %all-to-all-start.3 = ((bf16[64,4,2048]{2,1,0:T(4,128)(2,1)}), bf16[64,4,2048]{2,1,0:T(4,128)(2,1)S(1)}, u32[]{:S(2)}, u32[]{:S(2)}) async-start(bf16[64,4,2048]{2,1,0:T(4,128)(2,1)} %all_to_all.27), calls=%async_computation.3 | async-start | bytes 2097152 | tf_op jit(solution)/shard_map/all_to_all | solution.py:185
  328.0 0.8 reduce_sum.74
  328.8 26.8 %all-to-all-done.3 = bf16[64,4,2048]{2,1,0:T(4,128)(2,1)S(1)} async-done(((bf16[64,4,2048]{2,1,0:T(4,128)(2,1)}), bf16[64,4,2048]{2,1,0:T(4,128)(2,1)S(1)}, u32[]{:S(2)}, u32[]{:S(2)}) %all-to-all-start.3) | async-done | bytes 1048608 | tf_op jit(solution)/shard_map/all_to_all | solution.py:185
  355.9 1.1 gather_fusion
  357.6 4.2 %multiply_reduce_fusion = bf16[96,2048]{1,0:T(8,128)(2,1)} fusion(bf16[96,2,2048]{2,1,0:T(2,128)(2,1)S(1)} %reshape.217, pred[96,2]{1,0:T(8,128)(4,1)S(1)} %copy.90, f32[96,2]{1,0:T(8,128)S(1)} %copy.85), kind=kLoop, calls=%fused_computation.33 | loop fusion | flops 1376256 | bytes 1180608 | tf_op jit(solution)/shard_map/reduce_sum | solution.py:187
  (84 shorter events, 5.0 us)
Async XLA Ops:
  7.2 230.1 %copy-start = (bf16[2,128,2048]{2,1,0:T(8,128)(2,1)S(1)}, bf16[2,128,2048]{2,1,0:T(8,128)(2,1)}, u32[]{:S(2)}) copy-start(bf16[2,128,2048]{2,1,0:T(8,128)(2,1)} %param.22) | copy-start | bytes 3145732
  7.2 77.5 %all-gather.8.cloned.1.call-start = ((), (), s32[]{:S(2)}) async-start(), calls=%async_computation.4 | async-start | bytes 1769472 | tf_op jit(solution)/shard_map/all_gather | solution.py:22
  19.9 88.8 %all-gather.12.cloned.1.call-start = ((), (), s32[]{:S(2)}) async-start(), calls=%async_computation.6 | async-start | bytes 1769472 | tf_op jit(solution)/shard_map/all_gather | solution.py:22
  30.1 133.4 %all-gather.16.cloned.1.call-start = ((), (), s32[]{:S(2)}) async-start(), calls=%async_computation.8 | async-start | bytes 5242880 | tf_op jit(solution)/shard_map/all_gather | solution.py:169
  84.6 102.6 %all-gather.10.cloned.1.call-start = ((), (), s32[]{:S(2)}) async-start(), calls=%async_computation.5 | async-start | bytes 4718592 | tf_op jit(solution)/shard_map/all_gather | solution.py:22
  85.2 123.2 %all-gather.14.cloned.1.call-start = ((), (), s32[]{:S(2)}) async-start(), calls=%async_computation.7 | async-start | bytes 4718592 | tf_op jit(solution)/shard_map/all_gather | solution.py:22
  163.5 7.5 %copy-start.5 = (bf16[1024,2048]{1,0:T(8,128)(2,1)S(1)}, bf16[1024,2048]{1,0:T(8,128)(2,1)}, u32[]{:S(2)}) copy-start(bf16[1024,2048]{1,0:T(8,128)(2,1)} %all-gather.16.cloned.1.call-done) | copy-start | bytes 12582916
  163.5 7.5 %copy-start.6 = (bf16[1,2048,896]{2,1,0:T(8,128)(2,1)S(1)}, bf16[1,2048,896]{2,1,0:T(8,128)(2,1)}, u32[]{:S(2)}) copy-start(bf16[1,2048,896]{2,1,0:T(8,128)(2,1)} %param.27) | copy-start | bytes 11010052
  171.0 4.8 %copy-start.7 = (bf16[1,896,2048]{2,1,0:T(8,128)(2,1)S(1)}, bf16[1,896,2048]{2,1,0:T(8,128)(2,1)}, u32[]{:S(2)}) copy-start(bf16[1,896,2048]{2,1,0:T(8,128)(2,1)} %param.29) | copy-start | bytes 11010052
  181.9 5.2 %copy-start.1 = (bf16[192,2,128]{2,1,0:T(2,128)(2,1)S(1)}, bf16[192,2,128]{2,1,0:T(2,128)(2,1)}, u32[]{:S(2)}) copy-start(bf16[192,2,128]{2,1,0:T(2,128)(2,1)} %param.17) | copy-start | bytes 294916
  181.9 56.7 %all-to-all-start.2 = ((bf16[4,256,2048]{2,1,0:T(8,128)(2,1)}), bf16[4,256,2048]{2,1,0:T(8,128)(2,1)}, u32[]{:S(2)}, u32[]{:S(2)}) async-start(bf16[4,256,2048]{2,1,0:T(8,128)(2,1)} %bitcast.121), calls=%async_computation.2 | async-start | bytes 8388608 | tf_op jit(solution)/shard_map/all_to_all | solution.py:40
  212.3 24.4 %copy-start.4 = (f32[2]{0:T(128)S(1)}, f32[2]{0:T(128)}, u32[]{:S(2)}) copy-start(f32[2]{0:T(128)} %param.20) | copy-start | bytes 28
  212.3 24.7 %copy-start.3 = (f32[128]{0:T(128)S(1)}, f32[128]{0:T(128)}, u32[]{:S(2)}) copy-start(f32[128]{0:T(128)} %param.21) | copy-start | bytes 1540
  238.6 14.9 %all-to-all-start = ((bf16[4,48,2048]{2,1,0:T(8,128)(2,1)}), bf16[4,48,2048]{2,1,0:T(8,128)(2,1)S(1)}, u32[]{:S(2)}, u32[]{:S(2)}) async-start(bf16[4,48,2048]{2,1,0:T(8,128)(2,1)} %bitcast.30), calls=%async_computation | async-start | bytes 1572864 | tf_op jit(solution)/shard_map/all_to_all | solution.py:40
  245.7 82.2 %copy-start.2 = (f32[96,2]{0,1:T(2,128)S(1)}, f32[96,2]{0,1:T(2,128)}, u32[]{:S(2)}) copy-start(f32[96,2]{0,1:T(2,128)} %param.26) | copy-start | bytes 2308
  253.5 102.2 %all-to-all-start.3 = ((bf16[64,4,2048]{2,1,0:T(4,128)(2,1)}), bf16[64,4,2048]{2,1,0:T(4,128)(2,1)S(1)}, u32[]{:S(2)}, u32[]{:S(2)}) async-start(bf16[64,4,2048]{2,1,0:T(4,128)(2,1)} %all_to_all.27), calls=%async_computation.3 | async-start | bytes 2097152 | tf_op jit(solution)/shard_map/all_to_all | solution.py:185
Sparse Core Ops, SparseCore 0:
  20.0 43.5 all-gather.7
  65.3 43.2 all-gather.11
  110.5 52.9 all-gather.15
  165.2 18.7 all-gather.9
  185.6 18.7 all-gather.13
where the time goes:
time: 370 us; the launch traced here: 368 us
  waiting for transfers between devices  112 us (30%)
  starting transfers between devices  83.3 us (23%)
  blocking collectives  70 us (19%)
  local copies, waits for them, and re-layouts  41.2 us (11%)
  matrix products  24.3 us (7%)
  between operations  14.1 us (4%)
  other arithmetic  12.4 us (3%)
  loops' own time  10.7 us (3%)
    all_to_all x1, starting transfers between devices, body(): lax.all_to_all(expert_out, EP, split_axis=0, concat_axis=0, tiled=True)  74 us
    all_gather x1, waiting for transfers between devices, body(): inputs = lax.all_gather(received, 'tp', axis=0, tiled=True)  54.8 us
    all_to_all x1, blocking collectives, body(): lax.all_to_all(outbound, EP, split_axis=0, concat_axis=0, tiled=True)  47.2 us
    all_to_all x1, waiting for transfers between devices, body(): lax.all_to_all(expert_out, EP, split_axis=0, concat_axis=0, tiled=True)  26.8 us
    all_gather x4, waiting for transfers between devices, gather_in_order(): tiles = lax.all_gather(tiles, axes[k], axis=0, tiled=True)  23.5 us
    all_gather x2, blocking collectives, gather_in_order(): tiles = lax.all_gather(tiles, axes[k], axis=0, tiled=True)  22.8 us
    transpose x2, local copies, waits for them, and re-layouts, gather_in_order(): tiles.transpose(*turned, *range(len(order), tiles.ndim))  15.1 us
    another operation x1, loops' own time, body(): folded = lax.fori_loop(0, length // span, sweep, initial)  10.4 us
  transfers between devices with their start and end apart: 8, of which 4 were waited for; matrix products, arithmetic and copies ran while one was open for 19% of the time, Pallas kernels for 0%

commit v1 on v0

--- a/solution.py
+++ b/solution.py
@@ -166,7 +166,11 @@
     ).astype(jnp.bfloat16)
     outbound = jnp.dot(dispatch, normed_in, preferred_element_type=jnp.float32).astype(jnp.bfloat16)
     received = lax.all_to_all(outbound, EP, split_axis=0, concat_axis=0, tiled=True)
-    inputs = lax.all_gather(received, "tp", axis=0, tiled=True)
+    peers_2 = lax.axis_size("tp")
+    repeats = [peers_2 if d == 0 else 1 for d in range(received.ndim)]
+    inputs = lax.all_to_all(
+        jnp.tile(received, repeats), "tp", split_axis=0, concat_axis=0, tiled=True
+    )
     gate_proj = jnp.dot(inputs, gate_weight[0], preferred_element_type=jnp.float32)
     up_proj = jnp.dot(inputs, up_weight[0], preferred_element_type=jnp.float32)
     hidden_all = (jax.nn.silu(gate_proj) * up_proj).astype(jnp.bfloat16)

time: 370 us -> 349 us (0.943)
  waiting for transfers between devices: 112 us -> 79.8 us
  local copies, waits for them, and re-layouts: 41.2 us -> 45.7 us
    all_gather x1 -> x0, waiting for transfers between devices: 54.8 us -> none  [body(): inputs = lax.all_gather(received, 'tp', axis=0, tiled=True)]
    all_to_all x0 -> x1, waiting for transfers between devices: none -> 31.9 us  [body(): lax.all_to_all(jnp.tile(received, repeats), 'tp', split_axis=0, concat_ax...]
    all_gather x4, waiting for transfers between devices: 23.5 us -> 16.3 us  [gather_in_order(): tiles = lax.all_gather(tiles, axes[k], axis=0, tiled=True)]
    all_to_all x0 -> x1, starting transfers between devices: none -> 4.85 us  [body(): lax.all_to_all(jnp.tile(received, repeats), 'tp', split_axis=0, concat_ax...]
    another operation x2 -> x4, local copies, waits for them, and re-layouts: 0.19 us -> 4.09 us  [the longest x2 3.9 us: body(): jnp.tile(received, repeats)]
  transfers between devices with their start and end apart: 8 -> 8, of which waited for: 4 -> 4; matrix products, arithmetic and copies ran while one was open for 19% -> 22% of each run, Pallas kernels for 0% -> 0%
where the time goes in v1:
time: 349 us; the launch traced here: 347 us
  starting transfers between devices  86.3 us (25%)
  waiting for transfers between devices  79.8 us (23%)
  blocking collectives  70.1 us (20%)
  local copies, waits for them, and re-layouts  45.7 us (13%)
  matrix products  26.9 us (8%)
  between operations  14.1 us (4%)
  other arithmetic  13.5 us (4%)
  loops' own time  10.9 us (3%)
    all_to_all x1, starting transfers between devices, body(): lax.all_to_all(expert_out, EP, split_axis=0, concat_axis=0, tiled=True)  72.2 us
    all_to_all x1, blocking collectives, body(): lax.all_to_all(outbound, EP, split_axis=0, concat_axis=0, tiled=True)  47.3 us
    all_to_all x1, waiting for transfers between devices, body(): lax.all_to_all(jnp.tile(received, repeats), 'tp', split_axis=0, concat_ax...  31.9 us
    all_to_all x1, waiting for transfers between devices, body(): lax.all_to_all(expert_out, EP, split_axis=0, concat_axis=0, tiled=True)  25.7 us
    all_gather x2, blocking collectives, gather_in_order(): tiles = lax.all_gather(tiles, axes[k], axis=0, tiled=True)  22.8 us
    all_gather x4, waiting for transfers between devices, gather_in_order(): tiles = lax.all_gather(tiles, axes[k], axis=0, tiled=True)  16.3 us
    transpose x2, local copies, waits for them, and re-layouts, gather_in_order(): tiles.transpose(*turned, *range(len(order), tiles.ndim))  15.1 us
    another operation x1, loops' own time, body(): folded = lax.fori_loop(0, length // span, sweep, initial)  10.7 us
  transfers between devices with their start and end apart: 8, of which 4 were waited for; matrix products, arithmetic and copies ran while one was open for 22% of the time, Pallas kernels for 0%

profile of v1, /device:TPU:1, one launch (start us, length us, event | category | flops | bytes accessed | tf_op | source)
XLA Modules:
  0.0 347.3 jit_solution(563593959831310710)
XLA Ops:
  7.2 12.6 %all-gather = bf16[768,1,128]{2,0,1:T(8,128)(2,1)} all-gather(bf16[192,1,128]{2,0,1:T(8,128)(2,1)} %param.18), channel_id=2, replica_groups=mesh['ep_0'=8,'ep_1'=4,'ep_2'=2,'tp'=4] {'ep_1'}, dimensions={0}, use_global_device_ids=true | all-gather | bytes 245760 | tf_op jit(solution)/shard_map/all_gather | solution.py:22
  19.9 10.2 %all-gather.1 = bf16[768,1,128]{2,0,1:T(8,128)(2,1)} all-gather(bf16[192,1,128]{2,0,1:T(8,128)(2,1)} %param.19), channel_id=3, replica_groups=mesh['ep_0'=8,'ep_1'=4,'ep_2'=2,'tp'=4] {'ep_1'}, dimensions={0}, use_global_device_ids=true | all-gather | bytes 245760 | tf_op jit(solution)/shard_map/all_gather | solution.py:22
  30.2 0.8 copy.86
  32.3 0.7 compare_and_fusion
  33.1 1.2 fusion.22
  34.3 1.5 convolution_convert_fusion.1
  36.3 47.3 %all_to_all.40 = bf16[64,4,2048]{2,1,0:T(4,128)(2,1)} all-to-all(bf16[64,4,2048]{2,1,0:T(4,128)(2,1)S(1)} %all_to_all.27), channel_id=1, replica_groups=mesh['ep_0'=8,'ep_1'=4,'ep_2'=2,'tp'=4] {'ep_0','ep_1','ep_2'}, dimensions={0} | all-to-all | bytes 2097152 | tf_op jit(solution)/shard_map/all_to_all | solution.py:168
  83.6 1.4 tile.4
  85.0 2.5 tile.10
  87.5 4.8 %all-to-all-start.2 = ((bf16[4,256,2048]{2,1,0:T(8,128)(2,1)}), bf16[4,256,2048]{2,1,0:T(8,128)(2,1)}, u32[]{:S(2)}, u32[]{:S(2)}) async-start(bf16[4,256,2048]{2,1,0:T(8,128)(2,1)} %tile.10), calls=%async_computation.2 | async-start | bytes 8388608 | tf_op jit(solution)/shard_map/all_to_all | solution.py:171
  92.4 16.2 %all-gather.11.cloned.1.call-done = bf16[32,192,1,128]{3,1,2,0:T(8,128)(2,1)} async-done(((bf16[4,192,1,128]{3,1,2,0:T(8,128)(2,1)}), bf16[32,192,1,128]{3,1,2,0:T(8,128)(2,1)}) %all-gather.11.cloned.1.call-update) | async-done | bytes 1572880 | tf_op jit(solution)/shard_map/all_gather | solution.py:22
  108.7 31.9 %all-to-all-done.2 = bf16[4,256,2048]{2,1,0:T(8,128)(2,1)} async-done(((bf16[4,256,2048]{2,1,0:T(8,128)(2,1)}), bf16[4,256,2048]{2,1,0:T(8,128)(2,1)}, u32[]{:S(2)}, u32[]{:S(2)}) %all-to-all-start.2) | async-done | bytes 4194336 | tf_op jit(solution)/shard_map/all_to_all | solution.py:171
  140.6 7.5 %fusion.16 = f32[1024,896]{1,0:T(8,128)S(1)} fusion(bf16[1024,2048]{1,0:T(8,128)(2,1)} %bitcast.32, bf16[1,2048,896]{2,1,0:T(8,128)(2,1)} %param.28), kind=kOutput, calls=%fused_computation.26 | convolution fusion | flops 3758096384 | bytes 11534336 | tf_op jit(solution)/shard_map/dot_general | solution.py:175
  148.1 7.3 %multiply_convert_fusion = bf16[1024,896]{1,0:T(8,128)(2,1)S(1)} fusion(f32[1024,896]{1,0:T(8,128)S(1)} %fusion.16, bf16[1024,2048]{1,0:T(8,128)(2,1)} %bitcast.32, bf16[1,2048,896]{2,1,0:T(8,128)(2,1)S(1)} %copy-done.6), kind=kOutput, calls=%fused_computation.30 | convolution fusion | flops 3763601408 | bytes 13369344 | tf_op jit(solution)/shard_map/dot_general | solution.py:174
  155.5 6.1 %convolution_convert_fusion = bf16[1024,2048]{1,0:T(8,128)(2,1)} fusion(bf16[1024,896]{1,0:T(8,128)(2,1)S(1)} %multiply_convert_fusion, bf16[1,896,2048]{2,1,0:T(8,128)(2,1)S(1)} %copy-done.7), kind=kOutput, calls=%fused_computation.24 | convolution fusion | flops 3760193536 | bytes 9699328 | tf_op jit(solution)/shard_map/dot_general | solution.py:183
  161.5 5.2 %all-to-all-start.3 = ((bf16[4,256,2048]{2,1,0:T(8,128)(2,1)}), bf16[4,256,2048]{2,1,0:T(8,128)(2,1)}, u32[]{:S(2)}, u32[]{:S(2)}) async-start(bf16[4,256,2048]{2,1,0:T(8,128)(2,1)} %bitcast.122), calls=%async_computation.3 | async-start | bytes 8388608 | tf_op jit(solution)/shard_map/all_to_all | solution.py:40
  166.9 11.1 %copy.79 = bf16[8,4,2,192,1,128]{3,2,1,0,5,4:T(2,128)(2,1)} copy(bf16[8,4,2,192,1,128]{5,3,1,0,2,4:T(8,128)(2,1)} %bitcast.123) | data formatting | bytes 6291456 | tf_op jit(solution)/shard_map/transpose | solution.py:26
  178.0 9.8 %reshape_reshape_reshape.3 = bf16[12288,1,2,64]{0,3,2,1:T(8,128)(2,1)} reshape(bf16[8,4,2,192,1,128]{3,2,1,0,5,4:T(2,128)(2,1)} %copy.79) | data formatting | bytes 6291456 | tf_op jit(solution)/shard_map/reshape;reshape;reshape | solution.py:108
  187.9 3.9 %copy.81 = bf16[8,4,2,192,1,128]{5,3,2,1,0,4:T(8,128)(2,1)} copy(bf16[8,4,2,192,1,128]{5,3,1,0,2,4:T(8,128)(2,1)} %bitcast.125) | data formatting | bytes 6291456 | tf_op jit(solution)/shard_map/transpose | solution.py:26
  191.9 25.5 %while.17 = (s32[]{:T(128)}, f32[1,2,2,192]{3,1,2,0:T(2,128)S(1)}, f32[1,2,2,192]{3,1,2,0:T(2,128)S(1)}, f32[1,2,2,192,128]{4,3,2,1,0:T(8,128)S(1)}, s32[192]{0:...) while((s32[]{:T(128)}, f32[1,2,2,192]{3,1,2,0:T(2,128)S(1)}, ...), condition=%wide.region_5.6_spmd, body=%wide.region_0.5_spmd.sunk | while | flops 232147968 | bytes 8857645 | solution.py:128
  191.9 0.6 slice.57
  193.2 4.3 %conditional.2 = ((f32[1,2,2,192]{3,1,2,0:T(2,128)S(1)}, f32[1,2,2,192]{3,1,2,0:T(2,128)S(1)}, f32[1,2,2,192,128]{4,3,2,1,0:T(8,128)S(1)})) conditional(s32[]{:T(128)} %convert_element_type.91, (f32[1,2,2,192]{3,1,2,0:T(2,128)S(1)}, f32[1,2,2,192]{3,1,2,0:T(2,128)S(1)}, f32[1,2,2,192,128]{4,3,2,1,0:T(8,128)S(1)}) %tuple.61, (s32[]{:T(128)}, ...), branch_computations={%region_1.0_spmd, %region_2.4_spmd} | conditional | flops 232147968 | bytes 8857422 | solution.py:125
  193.4 1.6 fusion
  195.0 0.9 fusion.4
  195.9 1.5 fusion.3
  197.5 0.6 slice.57
  198.8 0.6 slice.57
  200.1 0.6 slice.57
  201.5 0.6 slice.57
  202.8 0.6 slice.57
  204.1 0.6 slice.57
  205.4 0.6 slice.57
  206.8 0.6 slice.57
  208.1 0.6 slice.57
  210.7 0.6 slice.57
  212.1 0.6 slice.57
  213.4 0.6 slice.57
  217.9 1.3 convolution_convert_fusion.2
  219.3 4.0 %all-to-all-start = ((bf16[4,48,2048]{2,1,0:T(8,128)(2,1)}), bf16[4,48,2048]{2,1,0:T(8,128)(2,1)S(1)}, u32[]{:S(2)}, u32[]{:S(2)}) async-start(bf16[4,48,2048]{2,1,0:T(8,128)(2,1)} %bitcast.30), calls=%async_computation | async-start | bytes 1572864 | tf_op jit(solution)/shard_map/all_to_all | solution.py:40
  223.3 3.1 reduce_sum.78
  226.3 1.2 all_to_all.32
  227.6 5.9 %all-to-all-done = bf16[4,48,2048]{2,1,0:T(8,128)(2,1)S(1)} async-done(((bf16[4,48,2048]{2,1,0:T(8,128)(2,1)}), bf16[4,48,2048]{2,1,0:T(8,128)(2,1)S(1)}, u32[]{:S(2)}, u32[]{:S(2)}) %all-to-all-start) | async-done | bytes 786464 | tf_op jit(solution)/shard_map/all_to_all | solution.py:40
  233.4 0.9 copy-done.1
  234.3 72.2 %all-to-all-start.4 = ((bf16[64,4,2048]{2,1,0:T(4,128)(2,1)}), bf16[64,4,2048]{2,1,0:T(4,128)(2,1)S(1)}, u32[]{:S(2)}, u32[]{:S(2)}) async-start(bf16[64,4,2048]{2,1,0:T(4,128)(2,1)} %all_to_all.32), calls=%async_computation.4 | async-start | bytes 2097152 | tf_op jit(solution)/shard_map/all_to_all | solution.py:189
  307.0 2.0 reduce_sum.74
  309.0 25.7 %all-to-all-done.4 = bf16[64,4,2048]{2,1,0:T(4,128)(2,1)S(1)} async-done(((bf16[64,4,2048]{2,1,0:T(4,128)(2,1)}), bf16[64,4,2048]{2,1,0:T(4,128)(2,1)S(1)}, u32[]{:S(2)}, u32[]{:S(2)}) %all-to-all-start.4) | async-done | bytes 1048608 | tf_op jit(solution)/shard_map/all_to_all | solution.py:189
  335.0 1.1 gather_fusion
  336.6 4.2 %multiply_reduce_fusion = bf16[96,2048]{1,0:T(8,128)(2,1)} fusion(bf16[96,2,2048]{2,1,0:T(2,128)(2,1)S(1)} %reshape.225, pred[96,2]{1,0:T(8,128)(4,1)S(1)} %copy.90, f32[96,2]{1,0:T(8,128)S(1)} %copy.85), kind=kLoop, calls=%fused_computation.33 | loop fusion | flops 1376256 | bytes 1180608 | tf_op jit(solution)/shard_map/reduce_sum | solution.py:191
  (84 shorter events, 6.4 us)
Async XLA Ops:
  7.2 210.8 %copy-start = (bf16[2,128,2048]{2,1,0:T(8,128)(2,1)S(1)}, bf16[2,128,2048]{2,1,0:T(8,128)(2,1)}, u32[]{:S(2)}) copy-start(bf16[2,128,2048]{2,1,0:T(8,128)(2,1)} %param.22) | copy-start | bytes 3145732
  7.2 77.8 %all-gather.7.cloned.1.call-start = ((), (), s32[]{:S(2)}) async-start(), calls=%async_computation.5 | async-start | bytes 1769472 | tf_op jit(solution)/shard_map/all_gather | solution.py:22
  19.9 88.8 %all-gather.11.cloned.1.call-start = ((), (), s32[]{:S(2)}) async-start(), calls=%async_computation.7 | async-start | bytes 1769472 | tf_op jit(solution)/shard_map/all_gather | solution.py:22
  30.1 136.7 %all-gather.9.cloned.1.call-start = ((), (), s32[]{:S(2)}) async-start(), calls=%async_computation.6 | async-start | bytes 4718592 | tf_op jit(solution)/shard_map/all_gather | solution.py:22
  87.5 53.1 %all-to-all-start.2 = ((bf16[4,256,2048]{2,1,0:T(8,128)(2,1)}), bf16[4,256,2048]{2,1,0:T(8,128)(2,1)}, u32[]{:S(2)}, u32[]{:S(2)}) async-start(bf16[4,256,2048]{2,1,0:T(8,128)(2,1)} %tile.10), calls=%async_computation.2 | async-start | bytes 8388608 | tf_op jit(solution)/shard_map/all_to_all | solution.py:171
  92.4 95.5 %all-gather.13.cloned.1.call-start = ((), (), s32[]{:S(2)}) async-start(), calls=%async_computation.8 | async-start | bytes 4718592 | tf_op jit(solution)/shard_map/all_gather | solution.py:22
  140.6 7.5 %copy-start.6 = (bf16[1,2048,896]{2,1,0:T(8,128)(2,1)S(1)}, bf16[1,2048,896]{2,1,0:T(8,128)(2,1)}, u32[]{:S(2)}) copy-start(bf16[1,2048,896]{2,1,0:T(8,128)(2,1)} %param.27) | copy-start | bytes 11010052
  148.1 7.4 %copy-start.7 = (bf16[1,896,2048]{2,1,0:T(8,128)(2,1)S(1)}, bf16[1,896,2048]{2,1,0:T(8,128)(2,1)}, u32[]{:S(2)}) copy-start(bf16[1,896,2048]{2,1,0:T(8,128)(2,1)} %param.29) | copy-start | bytes 11010052
  161.5 5.2 %copy-start.2 = (bf16[192,2,128]{2,1,0:T(2,128)(2,1)S(1)}, bf16[192,2,128]{2,1,0:T(2,128)(2,1)}, u32[]{:S(2)}) copy-start(bf16[192,2,128]{2,1,0:T(2,128)(2,1)} %param.17) | copy-start | bytes 294916
  161.5 57.7 %all-to-all-start.3 = ((bf16[4,256,2048]{2,1,0:T(8,128)(2,1)}), bf16[4,256,2048]{2,1,0:T(8,128)(2,1)}, u32[]{:S(2)}, u32[]{:S(2)}) async-start(bf16[4,256,2048]{2,1,0:T(8,128)(2,1)} %bitcast.122), calls=%async_computation.3 | async-start | bytes 8388608 | tf_op jit(solution)/shard_map/all_to_all | solution.py:40
  191.8 25.5 %copy-start.5 = (f32[2]{0:T(128)S(1)}, f32[2]{0:T(128)}, u32[]{:S(2)}) copy-start(f32[2]{0:T(128)} %param.20) | copy-start | bytes 28
  191.9 25.8 %copy-start.4 = (f32[128]{0:T(128)S(1)}, f32[128]{0:T(128)}, u32[]{:S(2)}) copy-start(f32[128]{0:T(128)} %param.21) | copy-start | bytes 1540
  219.3 14.2 %all-to-all-start = ((bf16[4,48,2048]{2,1,0:T(8,128)(2,1)}), bf16[4,48,2048]{2,1,0:T(8,128)(2,1)S(1)}, u32[]{:S(2)}, u32[]{:S(2)}) async-start(bf16[4,48,2048]{2,1,0:T(8,128)(2,1)} %bitcast.30), calls=%async_computation | async-start | bytes 1572864 | tf_op jit(solution)/shard_map/all_to_all | solution.py:40
  226.3 80.6 %copy-start.3 = (f32[96,2]{0,1:T(2,128)S(1)}, f32[96,2]{0,1:T(2,128)}, u32[]{:S(2)}) copy-start(f32[96,2]{0,1:T(2,128)} %param.26) | copy-start | bytes 2308
  233.4 0.9 copy-start.1
  234.3 100.4 %all-to-all-start.4 = ((bf16[64,4,2048]{2,1,0:T(4,128)(2,1)}), bf16[64,4,2048]{2,1,0:T(4,128)(2,1)S(1)}, u32[]{:S(2)}, u32[]{:S(2)}) async-start(bf16[64,4,2048]{2,1,0:T(4,128)(2,1)} %all_to_all.32), calls=%async_computation.4 | async-start | bytes 2097152 | tf_op jit(solution)/shard_map/all_to_all | solution.py:189
Sparse Core Ops, SparseCore 0:
  20.0 43.5 all-gather.6
  65.3 43.2 all-gather.10
  110.5 20.5 all-gather.8
  132.7 18.7 all-gather.12
